TPU v7x, 32 devices: a whole 2x2x4 slice. The times are simulated.
32 devices in a mesh: ep: 16 (over z, y, x), tp: 2 (over core).
Axes of the slice: x: 2, y: 2, z: 4, core: 2. Of those that a mesh axis runs over, the one named last changes fastest.
Arguments:
- tokens: bfloat16 [256, 2048], P('ep'), may hold values from -6 to 6
- mix_gain: float32 [2048], replicated, may hold values from 0.1 to 1.9
- w_query: bfloat16 [2048, 1024], P(None, 'tp'), may hold values from -0.125 to 0.125
- w_forget: bfloat16 [2048, 1024], P(None, 'tp'), may hold values from -0.125 to 0.125
- w_input: bfloat16 [2048, 1024], P(None, 'tp'), may hold values from -0.125 to 0.125
- w_outgate: bfloat16 [2048, 1024], P(None, 'tp'), may hold values from -0.125 to 0.125
- decay_floor: float32 [1024], P('tp'), may hold values from 0 to 0.9
- head_gain: float32 [128], replicated, may hold values from 0.1 to 1.9
- prev_state: float32 [256, 8, 128, 128], P('ep', 'tp'), may hold values from -4 to 4
- w_output: bfloat16 [1024, 2048], P('tp'), may hold values from -0.1875 to 0.1875
- moe_gain: float32 [2048], replicated, may hold values from 0.1 to 1.9
- route_ids: int32 [256, 2], P('ep'), may hold values from 0 to 7, all different within a row; in each aligned block of 16 rows (0 to 15, 16 to 31, ...) at most 16 rows name the same one
- route_logits: float32 [256, 2], P('ep'), may hold values from -6 to 6
- w_exp_gate: bfloat16 [16, 2048, 1536], P('ep', None, 'tp'), may hold values from -0.125 to 0.125
- w_exp_up: bfloat16 [16, 2048, 1536], P('ep', None, 'tp'), may hold values from -0.125 to 0.125
- w_exp_down: bfloat16 [16, 1536, 2048], P('ep', 'tp'), may hold values from -0.109375 to 0.109375
Outputs:
- layer_out: bfloat16 [256, 2048], P('ep')
- new_state: float32 [256, 8, 128, 128], P('ep', 'tp')
Inputs may be any that keep to these rules, and one draw needn't show every extreme that they name: `route_ids`: each row names 2 different experts; within the rows of one device no expert is named more than 16 times, and in every draw some expert is named exactly 16 times in some device's rows.
All inputs are finite; a program needn't handle non-finite values.
Results may differ from a plain program's by a relative error of at most 0.014.
Values may be sent and summed in bfloat16 or wider, within the bound.
A program may use at most 128 MiB of HBM per device.

v0:
```python
import jax
import jax.numpy as jnp
from jax import lax
from jax.sharding import PartitionSpec as P

TOP_K = 2
epsilon = 1e-06


def rms_scale(values, gains):
    return values * lax.rsqrt(jnp.mean(values * values, axis=-1, keepdims=True) + epsilon) * gains


def on_device(
    tokens,
    mix_gain,
    w_query,
    w_forget,
    w_input,
    w_outgate,
    decay_floor,
    head_gain,
    prev_state,
    w_output,
    moe_gain,
    route_ids,
    route_logits,
    w_exp_gate,
    w_exp_up,
    w_exp_down,
):
    seq_dev = tokens.shape[0]
    ep_size = lax.axis_size("ep")
    residual = tokens.astype(jnp.float32)
    normed = rms_scale(residual, mix_gain).astype(jnp.bfloat16)
    heads_dev = prev_state.shape[1]
    head_dim = prev_state.shape[2]
    head_width = heads_dev * head_dim
    query_part = jnp.dot(normed, w_query, preferred_element_type=jnp.float32).reshape(
        seq_dev, heads_dev, head_dim
    )
    forget_pre = jnp.dot(normed, w_forget, preferred_element_type=jnp.float32).reshape(
        seq_dev, heads_dev, head_dim
    )
    value_part = jnp.dot(normed, w_input, preferred_element_type=jnp.float32).reshape(
        seq_dev, heads_dev, head_dim
    )
    outgate_pre = jnp.dot(normed, w_outgate, preferred_element_type=jnp.float32).reshape(
        seq_dev, heads_dev, head_dim
    )
    floor_rate = decay_floor.reshape(heads_dev, head_dim)
    forget = floor_rate + (1.0 - floor_rate) * jax.nn.sigmoid(forget_pre)
    key_part = (1.0 - floor_rate) * jax.nn.sigmoid(-forget_pre)
    new_state = forget[..., None] * prev_state + key_part[..., None] * value_part[:, :, None, :]
    readout = jnp.sum(query_part[..., None] * new_state, axis=2)
    gated = (
        (rms_scale(readout, head_gain) * jax.nn.silu(outgate_pre))
        .reshape(seq_dev, head_width)
        .astype(jnp.bfloat16)
    )
    mixed_out = lax.psum(
        jnp.dot(gated, w_output, preferred_element_type=jnp.float32).astype(jnp.bfloat16), "tp"
    ).astype(jnp.float32)
    middle = (residual + mixed_out).astype(jnp.bfloat16)
    normed_two = rms_scale(middle.astype(jnp.float32), moe_gain).astype(jnp.bfloat16)
    experts = ep_size // 2
    capacity = min(seq_dev, max(2, 8 * seq_dev * TOP_K // experts))
    slot_total = ep_size * capacity
    pair_expert = route_ids.reshape(-1)
    onehot = (pair_expert[:, None] == jnp.arange(experts, dtype=jnp.int32)[None, :]).astype(
        jnp.int32
    )
    slot_rank = jnp.sum((jnp.cumsum(onehot, axis=0) - onehot) * onehot, axis=1)
    slot_ids = jnp.arange(slot_total, dtype=jnp.int32)
    slot_expert = slot_ids // capacity // 2
    slot_order = slot_ids % capacity
    matches = (slot_expert[:, None] == pair_expert[None, :]) & (
        slot_order[:, None] == slot_rank[None, :]
    )
    match_tok = jnp.any(matches.reshape(slot_total, seq_dev, TOP_K), axis=2)
    outgoing = (
        jnp.dot(match_tok.astype(jnp.bfloat16), normed_two, preferred_element_type=jnp.float32)
        .astype(jnp.bfloat16)
        .reshape(ep_size, capacity, -1)
    )
    arrived = lax.all_to_all(outgoing, "ep", split_axis=0, concat_axis=0, tiled=True)
    per_source = arrived.shape[1]
    slot_rows = arrived.reshape(ep_size * per_source, arrived.shape[2])
    gate_pre = jnp.dot(slot_rows, w_exp_gate[0], preferred_element_type=jnp.float32)
    up_pre = jnp.dot(slot_rows, w_exp_up[0], preferred_element_type=jnp.float32)
    activated = (jax.nn.silu(gate_pre) * up_pre).astype(jnp.bfloat16)
    partial_down = jnp.dot(activated, w_exp_down[0], preferred_element_type=jnp.float32)
    share = lax.psum_scatter(
        partial_down.astype(jnp.bfloat16), "tp", scatter_dimension=1, tiled=True
    )
    answer = share.reshape(ep_size, per_source, -1)
    returned = lax.all_to_all(answer, "ep", split_axis=0, concat_axis=0, tiled=True)
    returned = lax.all_gather(returned, "tp", axis=2, tiled=True)
    weights = jax.nn.sigmoid(route_logits - jnp.flip(route_logits, axis=1)).reshape(-1)
    combine = jnp.sum(
        (matches.astype(jnp.float32) * weights[None, :]).reshape(slot_total, seq_dev, TOP_K), axis=2
    ).T
    expert_sum = jnp.dot(
        combine,
        returned.reshape(slot_total, -1).astype(jnp.float32),
        precision=lax.Precision.HIGHEST,
    )
    layer_out = (middle.astype(jnp.float32) + expert_sum).astype(jnp.bfloat16)
    return (layer_out, new_state)


def solution(mesh):
    placed = (
        P("ep", None),
        P(),
        P(None, "tp"),
        P(None, "tp"),
        P(None, "tp"),
        P(None, "tp"),
        P("tp"),
        P(),
        P("ep", "tp", None, None),
        P("tp", None),
        P(),
        P("ep", None),
        P("ep", None),
        P("ep", None, "tp"),
        P("ep", None, "tp"),
        P("ep", "tp", None),
    )
    return jax.shard_map(
        on_device,
        mesh=mesh,
        in_specs=placed,
        out_specs=(P("ep", None), P("ep", "tp", None, None)),
        check_vma=False,
    )
```

profile of v0, /device:TPU:0, one launch (start us, length us, event | category | flops | bytes accessed | tf_op | source)
XLA Modules:
  0.0 138.2 jit_solution(3309153512424318484)
XLA Ops:
  7.2 0.0 copy-start
  7.2 0.0 copy-start.1
  7.2 0.0 copy-start.4
  7.2 0.0 all-reduce.2.cloned.1.call-start
  7.2 1.1 fusion.19
  8.4 2.1 %add_divide_fusion.1 = (f32[16,512]{1,0:T(8,128)S(1)}, f32[16,512]{1,0:T(8,128)S(1)}) fusion(bf16[2048,512]{1,0:T(8,128)(2,1)} %param.19, bf16[16,2048]{1,0:T(8,128)(2,1)} %param.16, f32[2048]{0:T(1024)} %param.17, f32[16]{0:T(128)S(1)} %add_rsqrt_fusion.2), kind=kOutput, calls=%fused_computation.37 | convolution fusion | flops 33726464 | bytes 2236480 | tf_op jit(solution)/shard_map/dot_general | solution.py:42
  10.5 0.7 broadcast_subtract_fusion
  11.2 2.1 %fusion.47 = f32[16,512]{1,0:T(8,128)S(1)} fusion(bf16[2048,512]{1,0:T(8,128)(2,1)} %param.18, bf16[16,2048]{1,0:T(8,128)(2,1)} %param.16, f32[2048]{0:T(1024)} %param.17, f32[16]{0:T(128)S(1)} %add_rsqrt_fusion.2), kind=kOutput, calls=%fused_computation.69 | convolution fusion | flops 33685504 | bytes 2203712 | tf_op jit(solution)/shard_map/dot_general | solution.py:39
  13.3 0.0 copy-done.1
  13.3 0.0 copy-done.4
  13.3 2.0 %fusion.43 = f32[16,512]{1,0:T(8,128)S(1)} fusion(bf16[2048,512]{1,0:T(8,128)(2,1)} %param.20, bf16[16,2048]{1,0:T(8,128)(2,1)S(1)} %copy-done.1, f32[2048]{0:T(1024)S(1)} %copy-done.4, f32[16]{0:T(128)S(1)} %add_rsqrt_fusion.2), kind=kOutput, calls=%fused_computation.67 | convolution fusion | flops 33685504 | bytes 2203712 | tf_op jit(solution)/shard_map/dot_general | solution.py:45
  15.4 0.0 copy-done.7
  15.4 0.0 copy-start.9
  15.4 8.1 %multiply_reduce_fusion = (f32[16,4,128]{2,1,0:T(4,128)S(1)}, f32[16,4,128,128]{3,2,1,0:T(8,128)}) fusion(f32[16,4,128]{2,1,0:T(4,128)S(1)} %mul.153, f32[16,4,128]{2,1,0:T(4,128)S(1)} %mul.161, f32[16,4,128]{2,1,0:T(4,128)S(1)} %bitcast.55, f32[16,4,128,128]{3,2,1,0:T(8,128)} %param.24, f32[16,4,128]{2,1,0:T(4,128)S(1)} %bitcast.54), kind=kLoop, calls=%fused_computation | loop fusion | flops 5234688 | bytes 8552448 | tf_op jit(solution)/shard_map/reduce_sum | solution.py:55
  23.6 0.0 copy-start.6
  23.6 0.1 multiply_reduce_fusion.1
  23.7 0.1 broadcast_multiply_fusion
  23.8 0.0 copy-done.9
  23.8 3.7 %convolution_convert_fusion.1 = bf16[16,2048]{1,0:T(8,128)(2,1)} fusion(bf16[512,2048]{1,0:T(8,128)(2,1)} %param.25, f32[2,8,4,128]{3,2,1,0:T(4,128)S(1)} %bitcast.56, f32[512]{0:T(512)S(1)} %broadcast_bitcast_fusion, bf16[2048,512]{1,0:T(8,128)(2,1)} %param.21, bf16[16,2048]{1,0:T(8,128)(2,1)S(1)} %copy-done.1, f32[2048]{0:T(1024)S(1)} %copy-done.4, ...), kind=kOutput, calls=%fused_computation.12 | convolution fusion | flops 67330048 | bytes 4368448 | tf_op jit(solution)/shard_map/dot_general | solution.py:62
  27.4 0.0 all-reduce.2.cloned.1.call-update
  27.5 0.0 reduce-scatter.2.cloned.1.call-start
  27.5 0.0 copy-done.5
  27.5 0.1 copy.24
  27.6 0.1 eq.53
  27.7 0.1 fusion.33
  27.8 0.1 reduce_window_sum.11
  27.8 0.2 select_reduce_fusion.1
  28.0 0.1 eq.57
  28.1 0.1 copy.25
  28.2 0.1 fusion.31
  28.3 19.8 %all-reduce.2.cloned.1.call-done = bf16[16,2048]{1,0:T(8,128)(2,1)} async-done(((bf16[16,2048]{1,0:T(8,128)(2,1)}), bf16[16,2048]{1,0:T(8,128)(2,1)}) %all-reduce.2.cloned.1.call-update) | async-done | bytes 65552 | tf_op jit(solution)/shard_map/psum | solution.py:61
  48.1 1.1 fusion.23
  49.2 0.0 copy-done.6
  49.2 1.3 convolution_convert_fusion
  50.5 33.3 %all_to_all.10 = bf16[16,16,2048]{2,1,0:T(8,128)(2,1)S(1)} all-to-all(bf16[16,16,2048]{2,1,0:T(8,128)(2,1)S(1)} %bitcast.49), channel_id=1, replica_groups=mesh['ep'=16,'tp'=2] {'ep'}, dimensions={0} | all-to-all | bytes 2097152 | tf_op jit(solution)/shard_map/all_to_all | solution.py:86
  83.9 1.0 copy-done.2
  84.9 0.0 copy-done.10
  84.9 1.9 %fusion.4 = f32[256,768]{1,0:T(8,128)} fusion(bf16[256,2048]{1,0:T(8,128)(2,1)S(1)} %bitcast.51, bf16[1,2048,768]{2,1,0:T(8,128)(2,1)S(1)} %copy-done.10), kind=kOutput, calls=%fused_computation.6 | convolution fusion | flops 805306368 | bytes 4980736 | tf_op jit(solution)/shard_map/dot_general | solution.py:89
  86.8 5.5 %fusion.6 = bf16[256,2048]{1,0:T(8,128)(2,1)} fusion(bf16[1,768,2048]{2,1,0:T(8,128)(2,1)S(1)} %copy-done, bf16[256,2048]{1,0:T(8,128)(2,1)} %bitcast.52, bf16[1,2048,768]{2,1,0:T(8,128)(2,1)} %param.30, f32[256,768]{1,0:T(8,128)} %fusion.4), kind=kOutput, calls=%fused_computation.9 | convolution fusion | flops 1612316672 | bytes 9175040 | tf_op jit(solution)/shard_map/dot_general | solution.py:92
  92.3 0.0 reduce-scatter.2.cloned.1.call-update
  92.4 0.0 all-gather.2.cloned.1.call-start
  92.4 6.8 %reduce-scatter.2.cloned.1.call-done = bf16[256,1024]{1,0:T(8,128)(2,1)} async-done(((bf16[256,2048]{1,0:T(8,128)(2,1)}), bf16[256,1024]{1,0:T(8,128)(2,1)}) %reduce-scatter.2.cloned.1.call-update) | async-done | bytes 524304 | tf_op jit(solution)/shard_map/reduce_scatter | solution.py:93
  99.3 22.4 %all_to_all.11 = bf16[16,16,1024]{2,1,0:T(8,128)(2,1)} all-to-all(bf16[16,16,1024]{2,1,0:T(8,128)(2,1)} %bitcast.53), channel_id=1, replica_groups=mesh['ep'=16,'tp'=2] {'ep'}, dimensions={0} | all-to-all | bytes 1048576 | tf_op jit(solution)/shard_map/all_to_all | solution.py:97
  121.6 0.0 all-gather.2.cloned.1.call-update
  121.7 0.0 copy-done.8
  121.7 0.1 select_reduce_fusion
  121.8 7.4 %all-gather.2.cloned.1.call-done = bf16[16,16,2048]{2,1,0:T(8,128)(2,1)} async-done(((bf16[16,16,1024]{2,1,0:T(8,128)(2,1)}), bf16[16,16,2048]{2,1,0:T(8,128)(2,1)}) %all-gather.2.cloned.1.call-update) | async-done | bytes 1048592 | tf_op jit(solution)/shard_map/all_gather | solution.py:98
  129.2 2.4 %fusion.9 = bf16[16,2048]{1,0:T(8,128)(2,1)} fusion(f32[256,16]{0,1:T(8,128)S(1)} %select_reduce_fusion, bf16[256,2048]{1,0:T(8,128)(2,1)} %bitcast.50, bf16[16,2048]{1,0:T(8,128)(2,1)S(1)} %copy-done.3, bf16[16,2048]{1,0:T(8,128)(2,1)S(1)} %copy-done.1), kind=kOutput, calls=%fused_computation.11 | convolution fusion | flops 100892672 | bytes 1261568 | tf_op jit(solution)/shard_map/dot_general | solution.py:103
  (22 shorter events, 0.2 us)
Async XLA Ops:
  7.2 79.6 %copy-start = (bf16[1,768,2048]{2,1,0:T(8,128)(2,1)S(1)}, bf16[1,768,2048]{2,1,0:T(8,128)(2,1)}, u32[]{:S(2)}) copy-start(bf16[1,768,2048]{2,1,0:T(8,128)(2,1)} %param.31) | copy-start | bytes 9437188
  7.2 6.1 %copy-start.1 = (bf16[16,2048]{1,0:T(8,128)(2,1)S(1)}, bf16[16,2048]{1,0:T(8,128)(2,1)}, u32[]{:S(2)}) copy-start(bf16[16,2048]{1,0:T(8,128)(2,1)} %param.16) | copy-start | bytes 196612
  7.2 6.1 %copy-start.4 = (f32[2048]{0:T(1024)S(1)}, f32[2048]{0:T(1024)}, u32[]{:S(2)}) copy-start(f32[2048]{0:T(1024)} %param.17) | copy-start | bytes 24580
  7.2 40.9 %all-reduce.2.cloned.1.call-start = ((), (), s32[]{:S(2)}) async-start(), calls=%async_computation.3 | async-start | bytes 131072 | tf_op jit(solution)/shard_map/psum | solution.py:61
  8.4 7.0 %copy-start.7 = (f32[512]{0:T(512)S(1)}, f32[512]{0:T(512)}, u32[]{:S(2)}) copy-start(f32[512]{0:T(512)} %param.22) | copy-start | bytes 6148
  15.4 8.3 %copy-start.9 = (f32[128]{0:T(128)S(1)}, f32[128]{0:T(128)}, u32[]{:S(2)}) copy-start(f32[128]{0:T(128)} %param.23) | copy-start | bytes 1540
  23.5 4.0 %copy-start.5 = (s32[16,2]{0,1:T(2,128)S(1)}, s32[16,2]{0,1:T(2,128)}, u32[]{:S(2)}) copy-start(s32[16,2]{0,1:T(2,128)} %param.27) | copy-start | bytes 388
  23.6 25.6 %copy-start.6 = (f32[2048]{0:T(1024)S(1)}, f32[2048]{0:T(1024)}, u32[]{:S(2)}) copy-start(f32[2048]{0:T(1024)} %param.26) | copy-start | bytes 24580
  27.5 71.8 %reduce-scatter.2.cloned.1.call-start = ((), (), s32[]{:S(2)}) async-start(), calls=%async_computation.4 | async-start | bytes 1572864 | tf_op jit(solution)/shard_map/reduce_scatter | solution.py:93
  48.1 36.9 %copy-start.10 = (bf16[1,2048,768]{2,1,0:T(8,128)(2,1)S(1)}, bf16[1,2048,768]{2,1,0:T(8,128)(2,1)}, u32[]{:S(2)}) copy-start(bf16[1,2048,768]{2,1,0:T(8,128)(2,1)} %param.29) | copy-start | bytes 9437188
  83.9 1.0 copy-start.2
  86.8 34.9 %copy-start.8 = (f32[16,2]{0,1:T(2,128)S(1)}, f32[16,2]{0,1:T(2,128)}, u32[]{:S(2)}) copy-start(f32[16,2]{0,1:T(2,128)} %param.28) | copy-start | bytes 388
  86.8 42.4 %copy-start.3 = (bf16[16,2048]{1,0:T(8,128)(2,1)S(1)}, bf16[16,2048]{1,0:T(8,128)(2,1)}, u32[]{:S(2)}) copy-start(bf16[16,2048]{1,0:T(8,128)(2,1)} %all-reduce.2.cloned.1.call-done) | copy-start | bytes 196612
  92.4 36.9 %all-gather.2.cloned.1.call-start = ((), (), s32[]{:S(2)}) async-start(), calls=%async_computation.5 | async-start | bytes 1572864 | tf_op jit(solution)/shard_map/all_gather | solution.py:98
Sparse Core Ops, SparseCore 0:
  27.6 20.4 all-reduce.1
  92.5 6.7 reduce-scatter.1
  121.8 7.4 all-gather.1
where the time goes:
time: 139 us; the launch traced here: 138 us
  blocking collectives  55.7 us (40%)
  waiting for transfers between devices  34.1 us (25%)
  matrix products  21 us (15%)
  between operations  14 us (10%)
  other arithmetic  11.7 us (8%)
  local copies, waits for them, and re-layouts  1.53 us (1%)
    all_to_all x1, blocking collectives, on_device(): lax.all_to_all(outgoing, 'ep', split_axis=0, concat_axis=0, tiled=True)  33.3 us
    all_to_all x1, blocking collectives, on_device(): lax.all_to_all(answer, 'ep', split_axis=0, concat_axis=0, tiled=True)  22.4 us
    psum x1, waiting for transfers between devices, on_device(): lax.psum(jnp.dot(gated, w_output, preferred_element_type=jnp.float32).ast...  19.8 us
    reduce_sum x1, other arithmetic, on_device(): readout = jnp.sum(query_part[..., None] * new_state, axis=2)  8.11 us
    all_gather x1, waiting for transfers between devices, on_device(): returned = lax.all_gather(returned, 'tp', axis=2, tiled=True)  7.45 us
    reduce_scatter x1, waiting for transfers between devices, on_device(): lax.psum_scatter(partial_down.astype(jnp.bfloat16), 'tp', scatter_dimensi...  6.85 us
    dot_general x1, matrix products, on_device(): jnp.dot(activated, w_exp_down[0], preferred_element_type=jnp.float32)  5.54 us
    dot_general x1, matrix products, on_device(): jnp.dot(gated, w_output, preferred_element_type=jnp.float32)  3.65 us
  transfers between devices with their start and end apart: 3, of which 3 were waited for; matrix products, arithmetic and copies ran while one was open for 1% of the time, Pallas kernels for 0%

commit v1 on v0

--- a/solution.py
+++ b/solution.py
@@ -5,6 +5,12 @@
 
 TOP_K = 2
 epsilon = 1e-06
+
+
+def _settle_copies(buf):
+    w1 = lax.all_gather(buf, "tp")
+    tile_out = jnp.sum(w1, axis=0)
+    return tile_out
 
 
 def rms_scale(values, gains):
@@ -58,8 +64,8 @@
         .reshape(seq_dev, head_width)
         .astype(jnp.bfloat16)
     )
-    mixed_out = lax.psum(
-        jnp.dot(gated, w_output, preferred_element_type=jnp.float32).astype(jnp.bfloat16), "tp"
+    mixed_out = _settle_copies(
+        jnp.dot(gated, w_output, preferred_element_type=jnp.float32).astype(jnp.bfloat16)
     ).astype(jnp.float32)
     middle = (residual + mixed_out).astype(jnp.bfloat16)
     normed_two = rms_scale(middle.astype(jnp.float32), moe_gain).astype(jnp.bfloat16)

time: 139 us -> 120 us (0.86)
  waiting for transfers between devices: 34.1 us -> 14.3 us
  blocking collectives: 55.7 us -> 59.2 us
  matrix products: 21 us -> 19.5 us
    psum x1 -> x0, waiting for transfers between devices: 19.8 us -> none  [on_device(): lax.psum(jnp.dot(gated, w_output, preferred_element_type=jnp.float32).ast...]
    all_gather x0 -> x1, blocking collectives: none -> 2.03 us  [_settle_copies(): w1 = lax.all_gather(buf, 'tp')]
    all_to_all x1, blocking collectives: 33.3 us -> 34.8 us  [on_device(): lax.all_to_all(outgoing, 'ep', split_axis=0, concat_axis=0, tiled=True)]
  transfers between devices with their start and end apart: 3 -> 2, of which waited for: 3 -> 2; matrix products, arithmetic and copies ran while one was open for 1% -> 0% of each run, Pallas kernels for 0% -> 0%
where the time goes in v1:
time: 120 us
  blocking collectives  59.2 us (49%)
  matrix products  19.5 us (16%)
  waiting for transfers between devices  14.3 us (12%)
  between operations  14.3 us (12%)
  other arithmetic  10.8 us (9%)
  local copies, waits for them, and re-layouts  1.53 us (1%)
    all_to_all x1, blocking collectives, on_device(): lax.all_to_all(outgoing, 'ep', split_axis=0, concat_axis=0, tiled=True)  34.8 us
    all_to_all x1, blocking collectives, on_device(): lax.all_to_all(answer, 'ep', split_axis=0, concat_axis=0, tiled=True)  22.4 us
    reduce_sum x1, other arithmetic, on_device(): readout = jnp.sum(query_part[..., None] * new_state, axis=2)  8.11 us
    all_gather x1, waiting for transfers between devices, on_device(): returned = lax.all_gather(returned, 'tp', axis=2, tiled=True)  7.45 us
    reduce_scatter x1, waiting for transfers between devices, on_device(): lax.psum_scatter(partial_down.astype(jnp.bfloat16), 'tp', scatter_dimensi...  6.82 us
    dot_general x1, matrix products, on_device(): jnp.dot(activated, w_exp_down[0], preferred_element_type=jnp.float32)  5.52 us
    dot_general x1, matrix products, on_device(): jnp.dot(gated, w_output, preferred_element_type=jnp.float32)  3.01 us
  transfers between devices with their start and end apart: 2, of which 2 were waited for; matrix products, arithmetic and copies ran while one was open for 0% of the time, Pallas kernels for 0%

profile of v1, /device:TPU:0, one launch (start us, length us, event | category | flops | bytes accessed | tf_op | source)
XLA Modules:
  0.0 119.6 jit_solution(7668793679527051703)
XLA Ops:
  7.2 0.0 copy-start
  7.2 0.0 copy-start.1
  7.2 0.0 copy-start.3
  7.2 0.0 reduce-scatter.2.cloned.1.call-start
  7.3 1.1 fusion.19
  8.4 0.0 copy-start.6
  8.4 2.1 %add_divide_fusion.1 = (f32[16,512]{1,0:T(8,128)S(1)}, f32[16,512]{1,0:T(8,128)S(1)}) fusion(bf16[2048,512]{1,0:T(8,128)(2,1)} %param.19, bf16[16,2048]{1,0:T(8,128)(2,1)} %param.16, f32[2048]{0:T(1024)} %param.17, f32[16]{0:T(128)S(1)} %add_rsqrt_fusion.2), kind=kOutput, calls=%fused_computation.37 | convolution fusion | flops 33726464 | bytes 2236480 | tf_op jit(solution)/shard_map/dot_general | solution.py:48
  10.6 0.7 broadcast_subtract_fusion
  11.2 2.1 %fusion.47 = f32[16,512]{1,0:T(8,128)S(1)} fusion(bf16[2048,512]{1,0:T(8,128)(2,1)} %param.18, bf16[16,2048]{1,0:T(8,128)(2,1)} %param.16, f32[2048]{0:T(1024)} %param.17, f32[16]{0:T(128)S(1)} %add_rsqrt_fusion.2), kind=kOutput, calls=%fused_computation.69 | convolution fusion | flops 33685504 | bytes 2203712 | tf_op jit(solution)/shard_map/dot_general | solution.py:45
  13.3 0.0 copy-done.1
  13.3 0.0 copy-done.3
  13.3 2.0 %fusion.43 = f32[16,512]{1,0:T(8,128)S(1)} fusion(bf16[2048,512]{1,0:T(8,128)(2,1)} %param.20, bf16[16,2048]{1,0:T(8,128)(2,1)S(1)} %copy-done.1, f32[2048]{0:T(1024)S(1)} %copy-done.3, f32[16]{0:T(128)S(1)} %add_rsqrt_fusion.2), kind=kOutput, calls=%fused_computation.67 | convolution fusion | flops 33685504 | bytes 2203712 | tf_op jit(solution)/shard_map/dot_general | solution.py:51
  15.4 0.0 copy-done.6
  15.4 0.0 copy-start.8
  15.4 8.1 %multiply_reduce_fusion = (f32[16,4,128]{2,1,0:T(4,128)S(1)}, f32[16,4,128,128]{3,2,1,0:T(8,128)}) fusion(f32[16,4,128]{2,1,0:T(4,128)S(1)} %mul.153, f32[16,4,128]{2,1,0:T(4,128)S(1)} %mul.161, f32[16,4,128]{2,1,0:T(4,128)S(1)} %bitcast.57, f32[16,4,128,128]{3,2,1,0:T(8,128)} %param.24, f32[16,4,128]{2,1,0:T(4,128)S(1)} %bitcast.56), kind=kLoop, calls=%fused_computation | loop fusion | flops 5234688 | bytes 8552448 | tf_op jit(solution)/shard_map/reduce_sum | solution.py:61
  23.6 0.0 copy-start.5
  23.6 0.1 multiply_reduce_fusion.1
  23.7 0.1 broadcast_multiply_fusion
  23.8 0.0 copy-done.8
  23.8 3.0 %convolution_convert_fusion.1 = bf16[16,2048]{1,0:T(8,128)(2,1)S(1)} fusion(bf16[512,2048]{1,0:T(8,128)(2,1)} %param.25, f32[2,8,4,128]{3,2,1,0:T(4,128)S(1)} %bitcast.58, f32[512]{0:T(512)S(1)} %broadcast_bitcast_fusion, bf16[2048,512]{1,0:T(8,128)(2,1)} %param.21, bf16[16,2048]{1,0:T(8,128)(2,1)S(1)} %copy-done.1, f32[2048]{0:T(1024)S(1)} %copy-done.3, ...), kind=kOutput, calls=%fused_computation.12 | convolution fusion | flops 67330048 | bytes 4368448 | tf_op jit(solution)/shard_map/dot_general | solution.py:68
  26.8 2.0 %all-gather = bf16[32,2048]{1,0:T(8,128)(2,1)S(1)} all-gather(bf16[16,2048]{1,0:T(8,128)(2,1)S(1)} %convolution_convert_fusion.1), channel_id=2, replica_groups=mesh['ep'=16,'tp'=2] {'tp'}, dimensions={0}, use_global_device_ids=true | all-gather | bytes 196608 | tf_op jit(solution)/shard_map/all_gather | solution.py:11
  28.9 0.1 fusion.23
  29.0 0.0 copy-done.4
  29.0 0.1 copy.24
  29.1 0.1 eq.53
  29.2 0.1 fusion.33
  29.3 0.1 reduce_window_sum.11
  29.3 0.2 select_reduce_fusion.1
  29.5 0.1 eq.57
  29.6 0.1 copy.25
  29.7 0.1 fusion.31
  29.8 0.0 copy-done.5
  29.8 0.5 convolution_convert_fusion
  30.3 34.8 %all_to_all.10 = bf16[16,16,2048]{2,1,0:T(8,128)(2,1)S(1)} all-to-all(bf16[16,16,2048]{2,1,0:T(8,128)(2,1)S(1)} %bitcast.50), channel_id=1, replica_groups=mesh['ep'=16,'tp'=2] {'ep'}, dimensions={0} | all-to-all | bytes 2097152 | tf_op jit(solution)/shard_map/all_to_all | solution.py:92
  65.1 1.0 copy-done.2
  66.1 0.0 copy-done.9
  66.1 1.9 %fusion.4 = f32[256,768]{1,0:T(8,128)} fusion(bf16[256,2048]{1,0:T(8,128)(2,1)S(1)} %bitcast.52, bf16[1,2048,768]{2,1,0:T(8,128)(2,1)S(1)} %copy-done.9), kind=kOutput, calls=%fused_computation.6 | convolution fusion | flops 805306368 | bytes 4980736 | tf_op jit(solution)/shard_map/dot_general | solution.py:95
  68.0 0.0 copy-done
  68.0 5.5 %fusion.6 = bf16[256,2048]{1,0:T(8,128)(2,1)} fusion(bf16[1,768,2048]{2,1,0:T(8,128)(2,1)S(1)} %copy-done, bf16[256,2048]{1,0:T(8,128)(2,1)} %bitcast.53, bf16[1,2048,768]{2,1,0:T(8,128)(2,1)} %param.30, f32[256,768]{1,0:T(8,128)} %fusion.4), kind=kOutput, calls=%fused_computation.9 | convolution fusion | flops 1612316672 | bytes 9175040 | tf_op jit(solution)/shard_map/dot_general | solution.py:98
  73.5 0.0 reduce-scatter.2.cloned.1.call-update
  73.5 0.0 all-gather.3.cloned.1.call-start
  73.6 6.8 %reduce-scatter.2.cloned.1.call-done = bf16[256,1024]{1,0:T(8,128)(2,1)} async-done(((bf16[256,2048]{1,0:T(8,128)(2,1)}), bf16[256,1024]{1,0:T(8,128)(2,1)}) %reduce-scatter.2.cloned.1.call-update) | async-done | bytes 524304 | tf_op jit(solution)/shard_map/reduce_scatter | solution.py:99
  80.4 22.4 %all_to_all.11 = bf16[16,16,1024]{2,1,0:T(8,128)(2,1)} all-to-all(bf16[16,16,1024]{2,1,0:T(8,128)(2,1)} %bitcast.55), channel_id=1, replica_groups=mesh['ep'=16,'tp'=2] {'ep'}, dimensions={0} | all-to-all | bytes 1048576 | tf_op jit(solution)/shard_map/all_to_all | solution.py:103
  102.8 0.0 all-gather.3.cloned.1.call-update
  102.8 0.0 copy-done.7
  102.8 0.1 select_reduce_fusion
  102.9 7.4 %all-gather.3.cloned.1.call-done = bf16[16,16,2048]{2,1,0:T(8,128)(2,1)} async-done(((bf16[16,16,1024]{2,1,0:T(8,128)(2,1)}), bf16[16,16,2048]{2,1,0:T(8,128)(2,1)}) %all-gather.3.cloned.1.call-update) | async-done | bytes 1048592 | tf_op jit(solution)/shard_map/all_gather | solution.py:104
  110.4 2.4 %fusion.9 = bf16[16,2048]{1,0:T(8,128)(2,1)} fusion(f32[256,16]{0,1:T(8,128)S(1)} %select_reduce_fusion, bf16[256,2048]{1,0:T(8,128)(2,1)} %bitcast.51, bf16[16,2048]{1,0:T(8,128)(2,1)S(1)} %reduce_sum.69, bf16[16,2048]{1,0:T(8,128)(2,1)S(1)} %copy-done.1), kind=kOutput, calls=%fused_computation.11 | convolution fusion | flops 100892672 | bytes 1261568 | tf_op jit(solution)/shard_map/dot_general | solution.py:109
  (19 shorter events, 0.2 us)
Async XLA Ops:
  7.2 60.8 %copy-start = (bf16[1,768,2048]{2,1,0:T(8,128)(2,1)S(1)}, bf16[1,768,2048]{2,1,0:T(8,128)(2,1)}, u32[]{:S(2)}) copy-start(bf16[1,768,2048]{2,1,0:T(8,128)(2,1)} %param.31) | copy-start | bytes 9437188
  7.2 6.2 %copy-start.1 = (bf16[16,2048]{1,0:T(8,128)(2,1)S(1)}, bf16[16,2048]{1,0:T(8,128)(2,1)}, u32[]{:S(2)}) copy-start(bf16[16,2048]{1,0:T(8,128)(2,1)} %param.16) | copy-start | bytes 196612
  7.2 6.2 %copy-start.3 = (f32[2048]{0:T(1024)S(1)}, f32[2048]{0:T(1024)}, u32[]{:S(2)}) copy-start(f32[2048]{0:T(1024)} %param.17) | copy-start | bytes 24580
  7.2 73.2 %reduce-scatter.2.cloned.1.call-start = ((), (), s32[]{:S(2)}) async-start(), calls=%async_computation.3 | async-start | bytes 1572864 | tf_op jit(solution)/shard_map/reduce_scatter | solution.py:99
  8.4 7.0 %copy-start.6 = (f32[512]{0:T(512)S(1)}, f32[512]{0:T(512)}, u32[]{:S(2)}) copy-start(f32[512]{0:T(512)} %param.22) | copy-start | bytes 6148
  15.4 8.3 %copy-start.8 = (f32[128]{0:T(128)S(1)}, f32[128]{0:T(128)}, u32[]{:S(2)}) copy-start(f32[128]{0:T(128)} %param.23) | copy-start | bytes 1540
  23.6 5.5 %copy-start.4 = (s32[16,2]{0,1:T(2,128)S(1)}, s32[16,2]{0,1:T(2,128)}, u32[]{:S(2)}) copy-start(s32[16,2]{0,1:T(2,128)} %param.27) | copy-start | bytes 388
  23.6 6.2 %copy-start.5 = (f32[2048]{0:T(1024)S(1)}, f32[2048]{0:T(1024)}, u32[]{:S(2)}) copy-start(f32[2048]{0:T(1024)} %param.26) | copy-start | bytes 24580
  29.7 36.4 %copy-start.9 = (bf16[1,2048,768]{2,1,0:T(8,128)(2,1)S(1)}, bf16[1,2048,768]{2,1,0:T(8,128)(2,1)}, u32[]{:S(2)}) copy-start(bf16[1,2048,768]{2,1,0:T(8,128)(2,1)} %param.29) | copy-start | bytes 9437188
  65.1 1.0 copy-start.2
  68.0 34.8 %copy-start.7 = (f32[16,2]{0,1:T(2,128)S(1)}, f32[16,2]{0,1:T(2,128)}, u32[]{:S(2)}) copy-start(f32[16,2]{0,1:T(2,128)} %param.28) | copy-start | bytes 388
  73.5 36.8 %all-gather.3.cloned.1.call-start = ((), (), s32[]{:S(2)}) async-start(), calls=%async_computation.4 | async-start | bytes 1572864 | tf_op jit(solution)/shard_map/all_gather | solution.py:104
Sparse Core Ops, SparseCore 0:
  73.7 6.7 reduce-scatter.1
  102.9 7.4 all-gather.2
